TPU v7x, 32 devices: a whole 2x2x4 slice. The times are simulated.
32 devices in a mesh: sp: 8 (over z, y), tp: 4 (over x, core).
Axes of the slice: x: 2, y: 2, z: 4, core: 2. Of those that a mesh axis runs over, the one named last changes fastest.
Arguments:
- stream: bfloat16 [2048, 2048], P('sp'), may hold values from -3 to 3
- first_group_queries: bfloat16 [2048, 512], P('sp', 'tp'), may hold values from -6 to 6
- first_group_keys: bfloat16 [2048, 512], P('sp', 'tp'), may hold values from -6 to 6
- first_group_values: bfloat16 [2048, 1024], P('sp', 'tp'), may hold values from -5.5 to 5.5
- first_gate_logits: bfloat16 [2048, 1024], P('sp', 'tp'), may hold values from -6 to 6
- first_decay_logits: bfloat16 [2048, 512], P('sp', 'tp'), may hold values from -4.75 to 14.5
- second_group_queries: bfloat16 [2048, 1024], P('sp', 'tp'), may hold values from -6 to 6
- second_group_keys: bfloat16 [2048, 1024], P('sp', 'tp'), may hold values from -6 to 6
- second_group_values: bfloat16 [2048, 1024], P('sp', 'tp'), may hold values from -5.5 to 5.5
- second_gate_logits: bfloat16 [2048, 1024], P('sp', 'tp'), may hold values from -6 to 6
- second_decay_logits: bfloat16 [2048, 1024], P('sp', 'tp'), may hold values from -4.75 to 14.5
- position_log_decay: float32 [2048], P('sp'), may hold values from -0.6932 to 0, as said below
- per_head_norm_gain: float32 [128], replicated, may hold values from 0.1 to 1.9
- first_output_weight: bfloat16 [1024, 2048], P('tp'), may hold values from -0.125 to 0.125
- second_output_weight: bfloat16 [1024, 2048], P('tp'), may hold values from -0.125 to 0.125
- feedforward_norm_gain: float32 [2048], replicated, may hold values from 0.1 to 1.9
- gate_weight: bfloat16 [2048, 5632], P('sp', 'tp'), may hold values from -0.125 to 0.125
- up_weight: bfloat16 [2048, 5632], P('sp', 'tp'), may hold values from -0.125 to 0.125
- down_weight: bfloat16 [5632, 2048], P('tp', 'sp'), may hold values from -0.078125 to 0.078125
Outputs:
- refined: bfloat16 [2048, 2048], P(('sp', 'tp'))
Inputs may be any that keep to these rules, and one draw needn't show every extreme that they name: `position_log_decay`: most positions carry 0.
All inputs are finite; a program needn't handle non-finite values.
Results may differ from a plain program's by a relative error of at most 0.018.
Values may be sent and summed in bfloat16 or wider, within the bound.
A program may use at most 64 MiB of HBM per device.

v0:
```python
import jax
import jax.numpy as jnp
from jax import lax
from jax.sharding import PartitionSpec as P

KEY_SIZE_FIRST = 64
KEY_SIZE_SECOND = 128
DV = 128
BLK = 64
decay_softness = 16.0
norm_eps = 1e-06
highest = lax.Precision.HIGHEST


def channel_log_decays(decay_logits, position_log_decay, key_channels):
    channel_log_decay = (
        jax.nn.log_sigmoid(decay_logits.astype(jnp.float32)) / decay_softness
        + position_log_decay[:, None]
    )
    return channel_log_decay.reshape(decay_logits.shape[0], -1, key_channels)


def one_way(query_matrix, key_matrix, value_matrix, channel_log_decay, start_state):
    length, heads, key_channels = query_matrix.shape
    value_width = value_matrix.shape[-1]
    block_count = length // BLK

    def blocks(member):
        return member.reshape(block_count, BLK, heads, member.shape[-1]).transpose(0, 2, 1, 3)

    query_blocks = blocks(query_matrix)
    key_blocks = blocks(key_matrix)
    value_blocks = blocks(value_matrix)
    running = jnp.cumsum(blocks(channel_log_decay), axis=2)
    block_last = running[:, :, -1:, :]
    query_in = query_blocks * jnp.exp(running)
    key_in = key_blocks * jnp.exp(-running)
    key_end = key_blocks * jnp.exp(block_last - running)
    places = jnp.arange(BLK, dtype=jnp.int32)
    lower = places[:, None] >= places[None, :]
    scores = jnp.where(
        lower, jnp.einsum("nhid,nhjd->nhij", query_in, key_in, precision=highest), 0.0
    )
    local_out = jnp.einsum("nhij,nhjv->nhiv", scores, value_blocks, precision=highest)

    def advance(states, inputs):
        query_part, key_part, value_part, last_part = inputs
        emitted = jnp.einsum("hid,hdv->hiv", query_part, states, precision=highest)
        states = states * jnp.exp(last_part)[:, 0, :, None] + jnp.einsum(
            "hjd,hjv->hdv", key_part, value_part, precision=highest
        )
        return (states, emitted)

    _, carried = lax.scan(advance, start_state, (query_in, key_end, value_blocks, block_last))
    return (local_out + carried).transpose(0, 2, 1, 3).reshape(length, heads, value_width)


def prepare_inputs(
    query_matrix, key_matrix, value_matrix, decay_logits, position_log_decay, key_channels
):
    length = query_matrix.shape[0]
    channel_log_decay = channel_log_decays(decay_logits, position_log_decay, key_channels)
    query_f = query_matrix.astype(jnp.float32).reshape(length, -1, key_channels)
    key_f = key_matrix.astype(jnp.float32).reshape(length, -1, key_channels)
    value_f = value_matrix.astype(jnp.float32).reshape(length, -1, DV)
    return (query_f, key_f, value_f, channel_log_decay)


def flipped(members):
    return tuple((jnp.flip(member, axis=0) for member in members))


def end_state(members):
    key_f, value_f, channel_log_decay = (members[1], members[2], members[3])
    totals = jnp.sum(channel_log_decay, axis=0)
    running = jnp.cumsum(channel_log_decay, axis=0)
    weighted = key_f * jnp.exp(totals[None] - running)
    states = jnp.einsum("thd,thv->hdv", weighted, value_f, precision=highest)
    return (totals, states)


def finish(forward, backward, gate_values, per_head_norm_gain):
    both = forward + backward
    scale = lax.rsqrt(jnp.mean(both * both, axis=-1, keepdims=True) + norm_eps)
    gated = (
        both
        * scale
        * per_head_norm_gain
        * jax.nn.silu(gate_values.astype(jnp.float32).reshape(both.shape))
    )
    return gated.reshape(both.shape[0], -1).astype(jnp.bfloat16)


def rms_rows(rows, feedforward_norm_gain):
    scale = lax.rsqrt(jnp.mean(rows * rows, axis=-1, keepdims=True) + norm_eps)
    return (rows * scale * feedforward_norm_gain).astype(jnp.bfloat16)


def per_device(
    stream,
    first_group_queries,
    first_group_keys,
    first_group_values,
    first_gate_logits,
    first_decay_logits,
    second_group_queries,
    second_group_keys,
    second_group_values,
    second_gate_logits,
    second_decay_logits,
    position_log_decay,
    per_head_norm_gain,
    first_output_weight,
    second_output_weight,
    feedforward_norm_gain,
    gate_weight,
    up_weight,
    down_weight,
):
    tok_rows = stream.shape[0]
    first_group = prepare_inputs(
        first_group_queries,
        first_group_keys,
        first_group_values,
        first_decay_logits,
        position_log_decay,
        KEY_SIZE_FIRST,
    )
    second_group = prepare_inputs(
        second_group_queries,
        second_group_keys,
        second_group_values,
        second_decay_logits,
        position_log_decay,
        KEY_SIZE_SECOND,
    )
    first_back = flipped(first_group)
    second_back = flipped(second_group)
    ahead_first = end_state(first_group)
    ahead_second = end_state(second_group)
    behind_first = end_state(first_back)
    behind_second = end_state(second_back)
    all_first, all_second = (
        lax.all_gather(ahead_first[0][None], "sp", axis=0, tiled=True),
        lax.all_gather(ahead_second[0][None], "sp", axis=0, tiled=True),
    )
    own_place = lax.axis_index("sp")

    def weights_for(all_logs, count):
        running = jnp.cumsum(all_logs, axis=0)
        own_end = running[own_place]
        own_before = own_end - all_logs[own_place]
        their_before = running - all_logs
        ranks = jnp.arange(count, dtype=jnp.int32)
        lower = (ranks < own_place)[:, None, None]
        higher = (ranks > own_place)[:, None, None]
        ahead = jnp.exp(jnp.where(lower, own_before - running, -jnp.inf))
        behind = jnp.exp(jnp.where(higher, their_before - own_end, -jnp.inf))
        return (ahead, behind)

    empty = (
        jnp.zeros_like(ahead_first[1]),
        jnp.zeros_like(ahead_first[1]),
        jnp.zeros_like(ahead_second[1]),
        jnp.zeros_like(ahead_second[1]),
    )
    pieces = (
        lax.all_gather(ahead_first[1][None].astype(jnp.bfloat16), "sp", axis=0, tiled=True).astype(
            jnp.float32
        ),
        lax.all_gather(behind_first[1][None].astype(jnp.bfloat16), "sp", axis=0, tiled=True).astype(
            jnp.float32
        ),
        lax.all_gather(ahead_second[1][None].astype(jnp.bfloat16), "sp", axis=0, tiled=True).astype(
            jnp.float32
        ),
        lax.all_gather(
            behind_second[1][None].astype(jnp.bfloat16), "sp", axis=0, tiled=True
        ).astype(jnp.float32),
    )
    count = pieces[0].shape[0]
    ahead_a, behind_a = weights_for(all_first, count)
    ahead_b, behind_b = weights_for(all_second, count)
    forward_first = one_way(
        first_group[0],
        first_group[1],
        first_group[2],
        first_group[3],
        empty[0] + jnp.einsum("nhd,nhdv->hdv", ahead_a, pieces[0], precision=highest),
    )
    backward_first = jnp.flip(
        one_way(
            first_back[0],
            first_back[1],
            first_back[2],
            first_back[3],
            empty[1] + jnp.einsum("nhd,nhdv->hdv", behind_a, pieces[1], precision=highest),
        ),
        0,
    )
    forward_second = one_way(
        second_group[0],
        second_group[1],
        second_group[2],
        second_group[3],
        empty[2] + jnp.einsum("nhd,nhdv->hdv", ahead_b, pieces[2], precision=highest),
    )
    backward_second = jnp.flip(
        one_way(
            second_back[0],
            second_back[1],
            second_back[2],
            second_back[3],
            empty[3] + jnp.einsum("nhd,nhdv->hdv", behind_b, pieces[3], precision=highest),
        ),
        0,
    )
    first_group_output = finish(
        forward_first, backward_first, first_gate_logits, per_head_norm_gain
    )
    second_group_output = finish(
        forward_second, backward_second, second_gate_logits, per_head_norm_gain
    )
    part_rows = tok_rows // lax.axis_size("tp")
    row_start = lax.axis_index("tp") * part_rows
    summed = lax.psum(
        (
            jnp.dot(first_group_output, first_output_weight, preferred_element_type=jnp.float32)
            + jnp.dot(second_group_output, second_output_weight, preferred_element_type=jnp.float32)
        ).astype(jnp.bfloat16),
        "tp",
    ).astype(jnp.float32)
    residual = stream.astype(jnp.float32) + summed
    normed_all = rms_rows(residual, feedforward_norm_gain)
    own_residual = lax.dynamic_slice_in_dim(residual, row_start, part_rows, 0)
    pieces = (
        lax.all_gather(gate_weight, "sp", axis=0, tiled=True),
        lax.all_gather(up_weight, "sp", axis=0, tiled=True),
    )
    gate_sum = jnp.dot(normed_all, pieces[0], preferred_element_type=jnp.float32)
    up_sum = jnp.dot(normed_all, pieces[1], preferred_element_type=jnp.float32)
    hidden = (jax.nn.silu(gate_sum) * up_sum).astype(jnp.bfloat16)
    down_whole = lax.all_gather(down_weight, "sp", axis=1, tiled=True)
    down_sum = lax.psum_scatter(
        jnp.dot(hidden, down_whole, preferred_element_type=jnp.float32).astype(jnp.bfloat16),
        "tp",
        scatter_dimension=0,
        tiled=True,
    ).astype(jnp.float32)
    return (own_residual + 0.5 * down_sum).astype(jnp.bfloat16)


def solution(mesh):
    in_specs = (
        P("sp", None),
        P("sp", "tp"),
        P("sp", "tp"),
        P("sp", "tp"),
        P("sp", "tp"),
        P("sp", "tp"),
        P("sp", "tp"),
        P("sp", "tp"),
        P("sp", "tp"),
        P("sp", "tp"),
        P("sp", "tp"),
        P("sp"),
        P(),
        P("tp", None),
        P("tp", None),
        P(),
        P("sp", "tp"),
        P("sp", "tp"),
        P("tp", "sp"),
    )
    out_specs = P(("sp", "tp"), None)
    return jax.shard_map(
        per_device, mesh=mesh, in_specs=in_specs, out_specs=out_specs, check_vma=False
    )
```

profile of v0, /device:TPU:0, one launch (start us, length us, event | category | flops | bytes accessed | tf_op | source)
XLA Modules:
  0.0 579.6 jit_solution(15194093987630395146)
XLA Ops:
  20.7 22.3 %all_gather.27 = f32[8,2,64]{2,1,0:T(2,128)S(1)} all-gather(f32[1,2,64]{2,1,0:T(2,128)S(1)} %broadcast_in_dim.108), channel_id=1, replica_groups=mesh['sp'=8,'tp'=4] {'sp'}, dimensions={0}, use_global_device_ids=true | all-gather | bytes 4608 | tf_op jit(solution)/shard_map/all_gather | solution.py:144
  46.7 32.8 %all-gather.1 = bf16[16,64,128]{2,1,0:T(8,128)(2,1)} all-gather(bf16[2,64,128]{2,1,0:T(8,128)(2,1)S(1)} %convolution_convert_fusion.4), channel_id=3, replica_groups=mesh['sp'=8,'tp'=4] {'sp'}, dimensions={0}, use_global_device_ids=true | all-gather | bytes 294912 | tf_op jit(solution)/shard_map/all_gather | solution.py:171
  80.6 1.6 fusion.71
  83.0 4.6 while.49
  92.3 32.8 %all-gather = bf16[16,64,128]{2,1,0:T(8,128)(2,1)} all-gather(bf16[2,64,128]{2,1,0:T(8,128)(2,1)S(1)} %convolution_convert_fusion.3), channel_id=2, replica_groups=mesh['sp'=8,'tp'=4] {'sp'}, dimensions={0}, use_global_device_ids=true | all-gather | bytes 294912 | tf_op jit(solution)/shard_map/all_gather | solution.py:168
  126.8 1.6 fusion.73
  128.4 2.3 while.48
  132.2 16.3 %all_gather.30 = f32[8,2,128]{2,1,0:T(2,128)S(1)} all-gather(f32[1,2,128]{2,1,0:T(2,128)S(1)} %bitcast.424), channel_id=1, replica_groups=mesh['sp'=8,'tp'=4] {'sp'}, dimensions={0}, use_global_device_ids=true | all-gather | bytes 9216 | tf_op jit(solution)/shard_map/all_gather | solution.py:145
  153.3 2.0 rev.40
  156.9 33.5 %all-gather.3 = bf16[16,128,128]{2,1,0:T(8,128)(2,1)} all-gather(bf16[2,128,128]{2,1,0:T(8,128)(2,1)S(1)} %convolution_convert_fusion.1), channel_id=5, replica_groups=mesh['sp'=8,'tp'=4] {'sp'}, dimensions={0}, use_global_device_ids=true | all-gather | bytes 589824 | tf_op jit(solution)/shard_map/all_gather | solution.py:177
  191.7 1.6 rev.37
  198.4 8.6 %while.51 = (s32[]{:T(128)}, f32[2,128,128]{2,1,0:T(8,128)S(1)}, f32[4,2,64,128]{3,2,1,0:T(8,128)}, f32[4,2,1,128]{3,1,2,0:T(2,128)S(1)}, f32[4,2,64,128]{3,2,1,...) while((s32[]{:T(128)}, f32[2,128,128]{2,1,0:T(8,128)S(1)}, ...), condition=%wide.region_26.27_spmd, body=%wide.region_25.26_spmd.sunk | while | flops 50397184 | bytes 660569 | solution.py:54
  212.0 33.2 %all-gather.2 = bf16[16,128,128]{2,1,0:T(8,128)(2,1)} all-gather(bf16[2,128,128]{2,1,0:T(8,128)(2,1)S(1)} %convolution_convert_fusion.2), channel_id=4, replica_groups=mesh['sp'=8,'tp'=4] {'sp'}, dimensions={0}, use_global_device_ids=true | all-gather | bytes 589824 | tf_op jit(solution)/shard_map/all_gather | solution.py:174
  248.7 2.2 fusion.48
  251.0 2.9 while.50
  260.7 33.2 %all-reduce.2.cloned.1.call-done = bf16[256,2048]{1,0:T(8,128)(2,1)} async-done(((bf16[256,2048]{1,0:T(8,128)(2,1)}), bf16[256,2048]{1,0:T(8,128)(2,1)}) %all-reduce.2.cloned.1.call-update) | async-done | bytes 1048592 | tf_op jit(solution)/shard_map/psum | solution.py:226
  293.9 2.0 convert_add_fusion
  295.9 56.1 %all-gather.8.cloned.1.call-done = bf16[2048,1408]{1,0:T(8,128)(2,1)} async-done(((bf16[256,1408]{1,0:T(8,128)(2,1)}), bf16[2048,1408]{1,0:T(8,128)(2,1)}) %all-gather.8.cloned.1.call-update) | async-done | bytes 5767184 | tf_op jit(solution)/shard_map/all_gather | solution.py:237
  352.0 6.3 %fusion.112 = f32[256,1408]{1,0:T(8,128)} fusion(bf16[2048,1408]{1,0:T(8,128)(2,1)} %all-gather.8.cloned.1.call-done, f32[2048]{0:T(1024)S(1)} %copy-done.33, f32[256]{0:T(256)S(1)} %add_rsqrt_fusion.2, bf16[256,2048]{1,0:T(8,128)(2,1)} %all-reduce.2.cloned.1.call-done, bf16[256,2048]{1,0:T(8,128)(2,1)} %param.27), kind=kOutput, calls=%fused_computation.189 | convolution fusion | flops 1479540736 | bytes 9315328 | tf_op jit(solution)/shard_map/dot_general | solution.py:240
  358.3 86.1 %all-gather.10.cloned.1.call-done = bf16[2048,1408]{1,0:T(8,128)(2,1)} async-done(((bf16[256,1408]{1,0:T(8,128)(2,1)}), bf16[2048,1408]{1,0:T(8,128)(2,1)}) %all-gather.10.cloned.1.call-update) | async-done | bytes 5767184 | tf_op jit(solution)/shard_map/all_gather | solution.py:238
  444.4 93.0 %all-gather.12.cloned.1.call-done = bf16[1408,2048]{1,0:T(8,128)(2,1)} async-done(((bf16[1408,256]{1,0:T(8,128)(2,1)}), bf16[1408,2048]{1,0:T(8,128)(2,1)}) %all-gather.12.cloned.1.call-update) | async-done | bytes 5767184 | tf_op jit(solution)/shard_map/all_gather | solution.py:243
  537.3 9.9 %convolution_convert_fusion = bf16[256,2048]{1,0:T(8,128)(2,1)} fusion(bf16[1408,2048]{1,0:T(8,128)(2,1)} %all-gather.12.cloned.1.call-done, bf16[2048,1408]{1,0:T(8,128)(2,1)} %all-gather.10.cloned.1.call-done, f32[256,1408]{1,0:T(8,128)} %fusion.112, f32[2048]{0:T(1024)S(1)} %copy-done.33, f32[256]{0:T(256)S(1)} %add_rsqrt_fusion.2, ...), kind=kOutput, calls=%fused_computation.60 | convolution fusion | flops 2958622720 | bytes 16131072 | tf_op jit(solution)/shard_map/dot_general | solution.py:245
  547.2 23.1 %reduce-scatter.2.cloned.1.call-done = bf16[64,2048]{1,0:T(8,128)(2,1)} async-done(((bf16[256,2048]{1,0:T(8,128)(2,1)}), bf16[64,2048]{1,0:T(8,128)(2,1)}) %reduce-scatter.2.cloned.1.call-update) | async-done | bytes 262160 | tf_op jit(solution)/shard_map/reduce_scatter | solution.py:244
  570.3 1.7 add_convert_fusion
  (284 shorter events, 71.8 us)
Async XLA Ops:
  7.4 248.9 %copy-start = (bf16[256,2048]{1,0:T(8,128)(2,1)S(1)}, bf16[256,2048]{1,0:T(8,128)(2,1)}, u32[]{:S(2)}) copy-start(bf16[256,2048]{1,0:T(8,128)(2,1)} %param.40) | copy-start | bytes 3145732
  7.4 5.3 copy-start.23
  7.4 6.3 %copy-start.3 = (bf16[256,256]{1,0:T(8,128)(2,1)S(1)}, bf16[256,256]{1,0:T(8,128)(2,1)}, u32[]{:S(2)}) copy-start(bf16[256,256]{1,0:T(8,128)(2,1)} %param.30) | copy-start | bytes 393220
  7.4 286.5 %all-reduce.2.cloned.1.call-start = ((), (), s32[]{:S(2)}) async-start(), calls=%async_computation.1 | async-start | bytes 2097152 | tf_op jit(solution)/shard_map/psum | solution.py:226
  8.4 6.9 %copy-start.18 = (bf16[256,256]{1,0:T(8,128)(2,1)S(1)}, bf16[256,256]{1,0:T(8,128)(2,1)}, u32[]{:S(2)}) copy-start(bf16[256,256]{1,0:T(8,128)(2,1)} %param.33) | copy-start | bytes 393220
  9.7 33.3 %copy-start.28 = (pred[8]{0:T(512)(128)(4,1)}, pred[8]{0:T(512)(128)(4,1)S(1)}, u32[]{:S(2)}) copy-start(pred[8]{0:T(512)(128)(4,1)S(1)} %get-tuple-element.377) | copy-start | bytes 28
  9.7 33.3 %copy-start.30 = (pred[8]{0:T(512)(128)(4,1)}, pred[8]{0:T(512)(128)(4,1)S(1)}, u32[]{:S(2)}) copy-start(pred[8]{0:T(512)(128)(4,1)S(1)} %get-tuple-element.378) | copy-start | bytes 28
  9.9 7.3 %copy-start.19 = (bf16[256,256]{1,0:T(8,128)(2,1)S(1)}, bf16[256,256]{1,0:T(8,128)(2,1)}, u32[]{:S(2)}) copy-start(bf16[256,256]{1,0:T(8,128)(2,1)} %param.34) | copy-start | bytes 393220
  12.8 32.6 %copy-start.4 = (f32[256,128]{0,1:T(8,128)}, f32[256,128]{0,1:T(8,128)S(1)}, u32[]{:S(2)}) copy-start(f32[256,128]{0,1:T(8,128)S(1)} %convert_element_type.93) | copy-start | bytes 393220
  12.8 5.6 copy-start.6
  88.2 37.0 %copy-start.12 = (f32[4,64,2,64]{1,0,3,2:T(4,128)S(1)}, f32[4,64,2,64]{1,0,3,2:T(4,128)}, u32[]{:S(2)}) copy-start(f32[4,64,2,64]{1,0,3,2:T(4,128)} %reshape_reshape.29) | copy-start | bytes 393220
  89.6 36.0 %copy-start.8 = (f32[4,64,2,64]{1,0,3,2:T(4,128)S(1)}, f32[4,64,2,64]{1,0,3,2:T(4,128)}, u32[]{:S(2)}) copy-start(f32[4,64,2,64]{1,0,3,2:T(4,128)} %reshape.253) | copy-start | bytes 393220
  89.6 36.1 %copy-start.9 = (f32[4,64,2,64]{1,0,3,2:T(4,128)S(1)}, f32[4,64,2,64]{1,0,3,2:T(4,128)}, u32[]{:S(2)}) copy-start(f32[4,64,2,64]{1,0,3,2:T(4,128)} %reshape.254) | copy-start | bytes 393220
  130.7 17.8 %copy-start.29 = (pred[8]{0:T(512)(128)(4,1)S(1)}, pred[8]{0:T(512)(128)(4,1)}, u32[]{:S(2)}) copy-start(pred[8]{0:T(512)(128)(4,1)} %copy-done.28) | copy-start | bytes 28
  130.7 17.8 %copy-start.31 = (pred[8]{0:T(512)(128)(4,1)S(1)}, pred[8]{0:T(512)(128)(4,1)}, u32[]{:S(2)}) copy-start(pred[8]{0:T(512)(128)(4,1)} %copy-done.30) | copy-start | bytes 28
  153.2 38.4 %copy-start.10 = (f32[256,256]{0,1:T(8,128)S(1)}, f32[256,256]{0,1:T(8,128)}, u32[]{:S(2)}) copy-start(f32[256,256]{0,1:T(8,128)} %convert_element_type.101) | copy-start | bytes 786436
  197.6 9.3 %copy-start.13 = (f32[4,2,64,64]{3,2,1,0:T(8,128)S(1)}, f32[4,2,64,64]{3,2,1,0:T(8,128)}, u32[]{:S(2)}) copy-start(f32[4,2,64,64]{3,2,1,0:T(8,128)} %convolution_select_fusion) | copy-start | bytes 393220
  209.8 36.8 %copy-start.1 = (f32[4,64,2,128]{1,0,3,2:T(4,128)S(1)}, f32[4,64,2,128]{1,0,3,2:T(4,128)}, u32[]{:S(2)}) copy-start(f32[4,64,2,128]{1,0,3,2:T(4,128)} %reshape.255) | copy-start | bytes 786436
  210.5 36.3 %copy-start.2 = (f32[4,64,2,128]{1,0,3,2:T(4,128)S(1)}, f32[4,64,2,128]{1,0,3,2:T(4,128)}, u32[]{:S(2)}) copy-start(f32[4,64,2,128]{1,0,3,2:T(4,128)} %reshape.256) | copy-start | bytes 786436
  258.7 93.3 %all-gather.8.cloned.1.call-start = ((), (), s32[]{:S(2)}) async-start(), calls=%async_computation.2 | async-start | bytes 6488064 | tf_op jit(solution)/shard_map/all_gather | solution.py:237
  259.3 185.1 %all-gather.10.cloned.1.call-start = ((), (), s32[]{:S(2)}) async-start(), calls=%async_computation.3 | async-start | bytes 6488064 | tf_op jit(solution)/shard_map/all_gather | solution.py:238
  259.8 277.5 %all-gather.12.cloned.1.call-start = ((), (), s32[]{:S(2)}) async-start(), calls=%async_computation.4 | async-start | bytes 6488064 | tf_op jit(solution)/shard_map/all_gather | solution.py:243
  260.4 91.6 %copy-start.33 = (f32[2048]{0:T(1024)S(1)}, f32[2048]{0:T(1024)}, u32[]{:S(2)}) copy-start(f32[2048]{0:T(1024)} %param.42) | copy-start | bytes 24580
  260.4 309.9 %reduce-scatter.2.cloned.1.call-start = ((), (), s32[]{:S(2)}) async-start(), calls=%async_computation.5 | async-start | bytes 1310720 | tf_op jit(solution)/shard_map/reduce_scatter | solution.py:244
  (15 other events, 37.4 us)
Sparse Core Ops, SparseCore 0:
  258.8 35.0 all-reduce.1
  547.4 22.9 reduce-scatter.1
Sparse Core Ops, SparseCore 1:
  261.3 90.6 all-gather.7
  354.1 90.2 all-gather.9
  446.3 91.0 all-gather.11
where the time goes:
time: 581 us; the launch traced here: 580 us
  waiting for transfers between devices  293 us (50%)
  blocking collectives  171 us (29%)
  matrix products  50.9 us (9%)
  local copies, waits for them, and re-layouts  33.3 us (6%)
  between operations  16.2 us (3%)
  other arithmetic  14.3 us (2%)
    all_gather x1, waiting for transfers between devices, per_device(): down_whole = lax.all_gather(down_weight, 'sp', axis=1, tiled=True)  93 us
    all_gather x1, waiting for transfers between devices, per_device(): lax.all_gather(up_weight, 'sp', axis=0, tiled=True)  86.1 us
    all_gather x1, waiting for transfers between devices, per_device(): lax.all_gather(gate_weight, 'sp', axis=0, tiled=True)  56.1 us
    all_gather x1, blocking collectives, per_device(): lax.all_gather(behind_second[1][None].astype(jnp.bfloat16), 'sp', axis=0,...  33.5 us
    psum x1, waiting for transfers between devices, per_device(): lax.psum((jnp.dot(first_group_output, first_output_weight, preferred_elem...  33.2 us
    all_gather x1, blocking collectives, per_device(): lax.all_gather(ahead_second[1][None].astype(jnp.bfloat16), 'sp', axis=0,...  33.2 us
    all_gather x1, blocking collectives, per_device(): lax.all_gather(ahead_first[1][None].astype(jnp.bfloat16), 'sp', axis=0, t...  32.8 us
    all_gather x1, blocking collectives, per_device(): lax.all_gather(behind_first[1][None].astype(jnp.bfloat16), 'sp', axis=0,...  32.8 us
  transfers between devices with their start and end apart: 5, of which 5 were waited for; matrix products, arithmetic and copies ran while one was open for 1% of the time, Pallas kernels for 0%

commit v1 on v0

--- a/solution.py
+++ b/solution.py
@@ -223,12 +223,17 @@
     )
     part_rows = tok_rows // lax.axis_size("tp")
     row_start = lax.axis_index("tp") * part_rows
-    summed = lax.psum(
-        (
-            jnp.dot(first_group_output, first_output_weight, preferred_element_type=jnp.float32)
-            + jnp.dot(second_group_output, second_output_weight, preferred_element_type=jnp.float32)
-        ).astype(jnp.bfloat16),
-        "tp",
+    summed = jnp.sum(
+        lax.all_gather(
+            (
+                jnp.dot(first_group_output, first_output_weight, preferred_element_type=jnp.float32)
+                + jnp.dot(
+                    second_group_output, second_output_weight, preferred_element_type=jnp.float32
+                )
+            ).astype(jnp.bfloat16),
+            "tp",
+        ),
+        axis=0,
     ).astype(jnp.float32)
     residual = stream.astype(jnp.float32) + summed
     normed_all = rms_rows(residual, feedforward_norm_gain)

time: 581 us -> 613 us (1.055)
  waiting for transfers between devices: 293 us -> 326 us
    all_gather x1, waiting for transfers between devices: 56.1 us -> 89.6 us  [per_device(): lax.all_gather(gate_weight, 'sp', axis=0, tiled=True)]
    psum x1 -> x0, waiting for transfers between devices: 33.2 us -> none  [per_device(): lax.psum((jnp.dot(first_group_output, first_output_weight, preferred_elem...]
    all_gather x0 -> x1, waiting for transfers between devices: none -> 30.8 us  [per_device(): lax.all_gather((jnp.dot(first_group_output, first_output_weight, preferre...]
  transfers between devices with their start and end apart: 5 -> 5, of which waited for: 5 -> 5; matrix products, arithmetic and copies ran while one was open for 1% -> 2% of each run, Pallas kernels for 0% -> 0%
where the time goes in v1:
time: 613 us; the launch traced here: 612 us
  waiting for transfers between devices  326 us (53%)
  blocking collectives  171 us (28%)
  matrix products  49.7 us (8%)
  local copies, waits for them, and re-layouts  33.3 us (5%)
  other arithmetic  17.3 us (3%)
  between operations  14.3 us (2%)
    all_gather x1, waiting for transfers between devices, per_device(): down_whole = lax.all_gather(down_weight, 'sp', axis=1, tiled=True)  93.2 us
    all_gather x1, waiting for transfers between devices, per_device(): lax.all_gather(gate_weight, 'sp', axis=0, tiled=True)  89.6 us
    all_gather x1, waiting for transfers between devices, per_device(): lax.all_gather(up_weight, 'sp', axis=0, tiled=True)  87.1 us
    all_gather x1, blocking collectives, per_device(): lax.all_gather(behind_second[1][None].astype(jnp.bfloat16), 'sp', axis=0,...  33.5 us
    all_gather x1, blocking collectives, per_device(): lax.all_gather(ahead_second[1][None].astype(jnp.bfloat16), 'sp', axis=0,...  33.2 us
    all_gather x1, blocking collectives, per_device(): lax.all_gather(ahead_first[1][None].astype(jnp.bfloat16), 'sp', axis=0, t...  32.8 us
    all_gather x1, blocking collectives, per_device(): lax.all_gather(behind_first[1][None].astype(jnp.bfloat16), 'sp', axis=0,...  32.8 us
    all_gather x1, waiting for transfers between devices, per_device(): lax.all_gather((jnp.dot(first_group_output, first_output_weight, preferre...  30.8 us
  transfers between devices with their start and end apart: 5, of which 5 were waited for; matrix products, arithmetic and copies ran while one was open for 2% of the time, Pallas kernels for 0%

profile of v1, /device:TPU:0, one launch (start us, length us, event | category | flops | bytes accessed | tf_op | source)
XLA Modules:
  0.0 612.3 jit_solution(18404025810015560495)
XLA Ops:
  19.9 22.3 %all_gather.33 = f32[8,2,64]{2,1,0:T(2,128)S(1)} all-gather(f32[1,2,64]{2,1,0:T(2,128)S(1)} %broadcast_in_dim.108), channel_id=1, replica_groups=mesh['sp'=8,'tp'=4] {'sp'}, dimensions={0}, use_global_device_ids=true | all-gather | bytes 4608 | tf_op jit(solution)/shard_map/all_gather | solution.py:144
  45.9 32.8 %all-gather.1 = bf16[16,64,128]{2,1,0:T(8,128)(2,1)} all-gather(bf16[2,64,128]{2,1,0:T(8,128)(2,1)S(1)} %convolution_convert_fusion.4), channel_id=3, replica_groups=mesh['sp'=8,'tp'=4] {'sp'}, dimensions={0}, use_global_device_ids=true | all-gather | bytes 294912 | tf_op jit(solution)/shard_map/all_gather | solution.py:171
  79.8 1.6 fusion.71
  82.2 4.6 while.49
  91.5 32.8 %all-gather = bf16[16,64,128]{2,1,0:T(8,128)(2,1)} all-gather(bf16[2,64,128]{2,1,0:T(8,128)(2,1)S(1)} %convolution_convert_fusion.3), channel_id=2, replica_groups=mesh['sp'=8,'tp'=4] {'sp'}, dimensions={0}, use_global_device_ids=true | all-gather | bytes 294912 | tf_op jit(solution)/shard_map/all_gather | solution.py:168
  125.9 1.6 fusion.73
  127.6 2.3 while.48
  131.3 16.3 %all_gather.36 = f32[8,2,128]{2,1,0:T(2,128)S(1)} all-gather(f32[1,2,128]{2,1,0:T(2,128)S(1)} %bitcast.426), channel_id=1, replica_groups=mesh['sp'=8,'tp'=4] {'sp'}, dimensions={0}, use_global_device_ids=true | all-gather | bytes 9216 | tf_op jit(solution)/shard_map/all_gather | solution.py:145
  152.4 2.0 rev.40
  156.1 33.5 %all-gather.3 = bf16[16,128,128]{2,1,0:T(8,128)(2,1)} all-gather(bf16[2,128,128]{2,1,0:T(8,128)(2,1)S(1)} %convolution_convert_fusion.1), channel_id=5, replica_groups=mesh['sp'=8,'tp'=4] {'sp'}, dimensions={0}, use_global_device_ids=true | all-gather | bytes 589824 | tf_op jit(solution)/shard_map/all_gather | solution.py:177
  197.5 8.6 %while.51 = (s32[]{:T(128)}, f32[2,128,128]{2,1,0:T(8,128)S(1)}, f32[4,2,64,128]{3,2,1,0:T(8,128)}, f32[4,2,1,128]{3,1,2,0:T(2,128)S(1)}, f32[4,2,64,128]{3,2,1,...) while((s32[]{:T(128)}, f32[2,128,128]{2,1,0:T(8,128)S(1)}, ...), condition=%wide.region_26.27_spmd, body=%wide.region_25.26_spmd.sunk | while | flops 50397184 | bytes 660569 | solution.py:54
  211.1 33.2 %all-gather.2 = bf16[16,128,128]{2,1,0:T(8,128)(2,1)} all-gather(bf16[2,128,128]{2,1,0:T(8,128)(2,1)S(1)} %convolution_convert_fusion.2), channel_id=4, replica_groups=mesh['sp'=8,'tp'=4] {'sp'}, dimensions={0}, use_global_device_ids=true | all-gather | bytes 589824 | tf_op jit(solution)/shard_map/all_gather | solution.py:174
  247.9 2.2 fusion.48
  250.2 2.9 while.50
  260.2 30.8 %all-gather.16.cloned.1.call-done = bf16[1024,2048]{1,0:T(8,128)(2,1)} async-done(((bf16[256,2048]{1,0:T(8,128)(2,1)}), bf16[1024,2048]{1,0:T(8,128)(2,1)}) %all-gather.16.cloned.1.call-update) | async-done | bytes 4194320 | tf_op jit(solution)/shard_map/all_gather | solution.py:227
  291.0 3.2 reduce_sum.81
  294.2 1.7 convert_add_fusion
  295.9 89.6 %all-gather.10.cloned.1.call-done = bf16[2048,1408]{1,0:T(8,128)(2,1)} async-done(((bf16[256,1408]{1,0:T(8,128)(2,1)}), bf16[2048,1408]{1,0:T(8,128)(2,1)}) %all-gather.10.cloned.1.call-update) | async-done | bytes 5767184 | tf_op jit(solution)/shard_map/all_gather | solution.py:242
  385.5 5.6 fusion.112
  391.1 87.1 %all-gather.12.cloned.1.call-done = bf16[2048,1408]{1,0:T(8,128)(2,1)} async-done(((bf16[256,1408]{1,0:T(8,128)(2,1)}), bf16[2048,1408]{1,0:T(8,128)(2,1)}) %all-gather.12.cloned.1.call-update) | async-done | bytes 5767184 | tf_op jit(solution)/shard_map/all_gather | solution.py:243
  478.2 93.2 %all-gather.14.cloned.1.call-done = bf16[1408,2048]{1,0:T(8,128)(2,1)} async-done(((bf16[1408,256]{1,0:T(8,128)(2,1)}), bf16[1408,2048]{1,0:T(8,128)(2,1)}) %all-gather.14.cloned.1.call-update) | async-done | bytes 5767184 | tf_op jit(solution)/shard_map/all_gather | solution.py:248
  571.5 9.2 %convolution_convert_fusion = bf16[256,2048]{1,0:T(8,128)(2,1)} fusion(bf16[1408,2048]{1,0:T(8,128)(2,1)} %all-gather.14.cloned.1.call-done, bf16[2048,1408]{1,0:T(8,128)(2,1)} %all-gather.12.cloned.1.call-done, f32[256,1408]{1,0:T(8,128)} %fusion.112, f32[2048]{0:T(1024)S(1)} %copy-done.34, f32[256]{0:T(256)S(1)} %add_rsqrt_fusion.2, ...), kind=kOutput, calls=%fused_computation.60 | convolution fusion | flops 2958622720 | bytes 16131072 | tf_op jit(solution)/shard_map/dot_general | solution.py:250
  580.7 23.1 %reduce-scatter.2.cloned.1.call-done = bf16[64,2048]{1,0:T(8,128)(2,1)} async-done(((bf16[256,2048]{1,0:T(8,128)(2,1)}), bf16[64,2048]{1,0:T(8,128)(2,1)}) %reduce-scatter.2.cloned.1.call-update) | async-done | bytes 262160 | tf_op jit(solution)/shard_map/reduce_scatter | solution.py:249
  603.9 1.9 add_convert_fusion
  (287 shorter events, 73.7 us)
Async XLA Ops:
  6.5 248.9 %copy-start = (bf16[256,2048]{1,0:T(8,128)(2,1)S(1)}, bf16[256,2048]{1,0:T(8,128)(2,1)}, u32[]{:S(2)}) copy-start(bf16[256,2048]{1,0:T(8,128)(2,1)} %param.40) | copy-start | bytes 3145732
  6.5 5.3 copy-start.24
  6.5 6.3 %copy-start.3 = (bf16[256,256]{1,0:T(8,128)(2,1)S(1)}, bf16[256,256]{1,0:T(8,128)(2,1)}, u32[]{:S(2)}) copy-start(bf16[256,256]{1,0:T(8,128)(2,1)} %param.30) | copy-start | bytes 393220
  6.5 284.4 %all-gather.16.cloned.1.call-start = ((), (), s32[]{:S(2)}) async-start(), calls=%async_computation.5 | async-start | bytes 5242880 | tf_op jit(solution)/shard_map/all_gather | solution.py:227
  7.6 6.9 %copy-start.19 = (bf16[256,256]{1,0:T(8,128)(2,1)S(1)}, bf16[256,256]{1,0:T(8,128)(2,1)}, u32[]{:S(2)}) copy-start(bf16[256,256]{1,0:T(8,128)(2,1)} %param.33) | copy-start | bytes 393220
  8.9 33.3 %copy-start.29 = (pred[8]{0:T(512)(128)(4,1)}, pred[8]{0:T(512)(128)(4,1)S(1)}, u32[]{:S(2)}) copy-start(pred[8]{0:T(512)(128)(4,1)S(1)} %get-tuple-element.377) | copy-start | bytes 28
  8.9 33.3 %copy-start.31 = (pred[8]{0:T(512)(128)(4,1)}, pred[8]{0:T(512)(128)(4,1)S(1)}, u32[]{:S(2)}) copy-start(pred[8]{0:T(512)(128)(4,1)S(1)} %get-tuple-element.378) | copy-start | bytes 28
  9.1 7.3 %copy-start.20 = (bf16[256,256]{1,0:T(8,128)(2,1)S(1)}, bf16[256,256]{1,0:T(8,128)(2,1)}, u32[]{:S(2)}) copy-start(bf16[256,256]{1,0:T(8,128)(2,1)} %param.34) | copy-start | bytes 393220
  11.9 32.6 %copy-start.4 = (f32[256,128]{0,1:T(8,128)}, f32[256,128]{0,1:T(8,128)S(1)}, u32[]{:S(2)}) copy-start(f32[256,128]{0,1:T(8,128)S(1)} %convert_element_type.95) | copy-start | bytes 393220
  12.0 5.6 copy-start.6
  87.4 37.0 %copy-start.13 = (f32[4,64,2,64]{1,0,3,2:T(4,128)S(1)}, f32[4,64,2,64]{1,0,3,2:T(4,128)}, u32[]{:S(2)}) copy-start(f32[4,64,2,64]{1,0,3,2:T(4,128)} %reshape_reshape.29) | copy-start | bytes 393220
  88.8 36.0 %copy-start.9 = (f32[4,64,2,64]{1,0,3,2:T(4,128)S(1)}, f32[4,64,2,64]{1,0,3,2:T(4,128)}, u32[]{:S(2)}) copy-start(f32[4,64,2,64]{1,0,3,2:T(4,128)} %reshape.254) | copy-start | bytes 393220
  88.8 36.1 %copy-start.10 = (f32[4,64,2,64]{1,0,3,2:T(4,128)S(1)}, f32[4,64,2,64]{1,0,3,2:T(4,128)}, u32[]{:S(2)}) copy-start(f32[4,64,2,64]{1,0,3,2:T(4,128)} %reshape.255) | copy-start | bytes 393220
  129.9 17.8 %copy-start.30 = (pred[8]{0:T(512)(128)(4,1)S(1)}, pred[8]{0:T(512)(128)(4,1)}, u32[]{:S(2)}) copy-start(pred[8]{0:T(512)(128)(4,1)} %copy-done.29) | copy-start | bytes 28
  129.9 17.8 %copy-start.32 = (pred[8]{0:T(512)(128)(4,1)S(1)}, pred[8]{0:T(512)(128)(4,1)}, u32[]{:S(2)}) copy-start(pred[8]{0:T(512)(128)(4,1)} %copy-done.31) | copy-start | bytes 28
  152.4 38.4 %copy-start.11 = (f32[256,256]{0,1:T(8,128)S(1)}, f32[256,256]{0,1:T(8,128)}, u32[]{:S(2)}) copy-start(f32[256,256]{0,1:T(8,128)} %convert_element_type.103) | copy-start | bytes 786436
  196.8 9.3 %copy-start.14 = (f32[4,2,64,64]{3,2,1,0:T(8,128)S(1)}, f32[4,2,64,64]{3,2,1,0:T(8,128)}, u32[]{:S(2)}) copy-start(f32[4,2,64,64]{3,2,1,0:T(8,128)} %convolution_select_fusion) | copy-start | bytes 393220
  208.9 36.8 %copy-start.1 = (f32[4,64,2,128]{1,0,3,2:T(4,128)S(1)}, f32[4,64,2,128]{1,0,3,2:T(4,128)}, u32[]{:S(2)}) copy-start(f32[4,64,2,128]{1,0,3,2:T(4,128)} %reshape.256) | copy-start | bytes 786436
  209.7 36.3 %copy-start.2 = (f32[4,64,2,128]{1,0,3,2:T(4,128)S(1)}, f32[4,64,2,128]{1,0,3,2:T(4,128)}, u32[]{:S(2)}) copy-start(f32[4,64,2,128]{1,0,3,2:T(4,128)} %reshape.257) | copy-start | bytes 786436
  257.9 127.6 %all-gather.10.cloned.1.call-start = ((), (), s32[]{:S(2)}) async-start(), calls=%async_computation.1 | async-start | bytes 6488064 | tf_op jit(solution)/shard_map/all_gather | solution.py:242
  258.6 219.6 %all-gather.12.cloned.1.call-start = ((), (), s32[]{:S(2)}) async-start(), calls=%async_computation.2 | async-start | bytes 6488064 | tf_op jit(solution)/shard_map/all_gather | solution.py:243
  259.4 312.1 %all-gather.14.cloned.1.call-start = ((), (), s32[]{:S(2)}) async-start(), calls=%async_computation.3 | async-start | bytes 6488064 | tf_op jit(solution)/shard_map/all_gather | solution.py:248
  259.9 343.9 %reduce-scatter.2.cloned.1.call-start = ((), (), s32[]{:S(2)}) async-start(), calls=%async_computation.4 | async-start | bytes 1310720 | tf_op jit(solution)/shard_map/reduce_scatter | solution.py:249
  294.2 91.4 %copy-start.34 = (f32[2048]{0:T(1024)S(1)}, f32[2048]{0:T(1024)}, u32[]{:S(2)}) copy-start(f32[2048]{0:T(1024)} %param.42) | copy-start | bytes 24580
  (16 other events, 40.5 us)
Sparse Core Ops, SparseCore 0:
  258.0 32.9 all-gather.15
  293.2 92.3 all-gather.9
  387.7 90.4 all-gather.11
  480.1 91.2 all-gather.13
  580.8 22.9 reduce-scatter.1
